TPU v7x, 512 devices: a whole 4x8x8 slice. The times are simulated.
512 devices in a mesh: ep: 128 (over z, y, core), tp: 4 (over x).
Axes of the slice: x: 4, y: 8, z: 8, core: 2. Of those that a mesh axis runs over, the one named last changes fastest.
Arguments:
- tokens: bfloat16 [8192, 1024], P('ep', 'tp'), may hold values from -6 to 6
- conv_state: bfloat16 [8192, 3, 512], P('ep', None, 'tp'), may hold values from -6 to 6
- lru_state: float32 [8192, 512], P('ep', 'tp'), may hold values from -6 to 6
- mix_gain: bfloat16 [1024], replicated, may hold values from 0.099609375 to 1.8984375
- ffn_gain: bfloat16 [1024], replicated, may hold values from 0.099609375 to 1.8984375
- w_branch: bfloat16 [1024, 512], P(None, 'tp'), may hold values from -0.1875 to 0.1875
- w_gate: bfloat16 [1024, 512], P(None, 'tp'), may hold values from -0.1875 to 0.1875
- conv_taps: bfloat16 [4, 512], P(None, 'tp'), may hold values from -3 to 3
- w_recur: bfloat16 [8, 64, 64], P('tp'), may hold values from -0.75 to 0.75
- w_inject: bfloat16 [8, 64, 64], P('tp'), may hold values from -0.75 to 0.75
- lru_lambda: float32 [512], P('tp'), may hold values from 2 to 7
- w_out: bfloat16 [512, 1024], P('tp'), may hold values from -0.25 to 0.25
- expert_gate: bfloat16 [128, 1024, 2560], P('ep', None, 'tp'), may hold values from -0.1875 to 0.1875
- expert_up: bfloat16 [128, 1024, 2560], P('ep', None, 'tp'), may hold values from -0.1875 to 0.1875
- expert_down: bfloat16 [128, 2560, 1024], P('ep', 'tp'), may hold values from -0.125 to 0.125
- route_ids: int32 [8192, 2], P('ep'), may hold values from 0 to 127, all different within a row; in each aligned block of 64 rows (0 to 63, 64 to 127, ...) at most 2 rows name the same one
- route_weight: float32 [8192, 2], P('ep'), may hold values from 0.2 to 1
Outputs:
- mixed: bfloat16 [8192, 1024], P('ep', 'tp')
- state_out: float32 [8192, 512], P('ep', 'tp')
Inputs may be any that keep to these rules, and one draw needn't show every extreme that they name: `route_ids`: each row names 2 different experts. Among the 64 rows of one device no expert is named more than 2 times, and in every draw some expert is named exactly 2 times by them.
All inputs are finite; a program needn't handle non-finite values.
Results may differ from a plain program's by a relative error of at most 0.015.
Values may be sent and summed in bfloat16 or wider, within the bound.
A program may use at most 64 MiB of HBM per device.

v0:
```python
import jax
import jax.numpy as jnp
from jax import lax
from jax.sharding import PartitionSpec as P

EPS = 1e-06
LRU_SCALE = 8.0


def joined_along(pieces, dim):
    pieces = jnp.moveaxis(pieces, 0, dim)
    lengths = pieces.shape
    return pieces.reshape(*lengths[:dim], lengths[dim] * lengths[dim + 1], *lengths[dim + 2 :])


def sent_to_all(x, axis):
    count = lax.axis_size(axis)
    return lax.all_to_all(jnp.broadcast_to(x[None], (count, *x.shape)), axis, 0, 0, tiled=True)


def gathered_copies(x, axis, dim):
    return joined_along(sent_to_all(x, axis), dim)


def in_blocks(x, dim, count):
    lengths = x.shape
    pieces = x.reshape(*lengths[:dim], count, lengths[dim] // count, *lengths[dim + 1 :])
    return jnp.moveaxis(pieces, dim, 0)


def sent_and_summed(x, axis, dim):
    pieces = in_blocks(x, dim, lax.axis_size(axis))
    arrived = lax.all_to_all(pieces, axis, split_axis=0, concat_axis=0, tiled=True)
    return arrived.astype(jnp.float32).sum(axis=0)


def rms_rows(rows, gain):
    values = rows.astype(jnp.float32)
    scaled = values * lax.rsqrt(jnp.mean(values * values, axis=-1, keepdims=True) + EPS)
    return (scaled * gain.astype(jnp.float32)).astype(jnp.bfloat16)


def body(
    tokens,
    conv_state,
    lru_state,
    mix_gain,
    ffn_gain,
    w_branch,
    w_gate,
    conv_taps,
    w_recur,
    w_inject,
    lru_lambda,
    w_out,
    expert_gate,
    expert_up,
    expert_down,
    route_ids,
    route_weight,
):
    seqs = tokens.shape[0]
    whole = gathered_copies(tokens, "tp", 1)
    normed = rms_rows(whole, mix_gain)
    branch = jnp.dot(normed, w_branch, preferred_element_type=jnp.float32).astype(jnp.bfloat16)
    gate_in = jnp.dot(normed, w_gate, preferred_element_type=jnp.float32).astype(jnp.bfloat16)
    window = jnp.concatenate([conv_state, branch[:, None, :]], axis=1).astype(jnp.float32)
    conv_out = jnp.sum(window * conv_taps.astype(jnp.float32)[None], axis=1)
    heads_here = w_recur.shape[0]
    head_width = w_recur.shape[1]
    conv_heads = conv_out.astype(jnp.bfloat16).reshape(seqs, heads_here, head_width)
    recur = jax.nn.sigmoid(
        jnp.einsum("nhi,hij->nhj", conv_heads, w_recur, preferred_element_type=jnp.float32).reshape(
            seqs, -1
        )
    )
    inject = jax.nn.sigmoid(
        jnp.einsum(
            "nhi,hij->nhj", conv_heads, w_inject, preferred_element_type=jnp.float32
        ).reshape(seqs, -1)
    )
    log_decay = -LRU_SCALE * recur * jax.nn.softplus(-lru_lambda)
    state_out = (
        jnp.exp(log_decay) * lru_state + jnp.sqrt(-jnp.expm1(2.0 * log_decay)) * inject * conv_out
    )
    lru_out = (state_out * jax.nn.gelu(gate_in.astype(jnp.float32))).astype(jnp.bfloat16)
    partial_value = jnp.dot(lru_out, w_out, preferred_element_type=jnp.float32)
    partial_value = lax.optimization_barrier(partial_value.astype(jnp.bfloat16)).astype(jnp.float32)
    mix_out = sent_and_summed(partial_value.astype(jnp.bfloat16), "tp", 1).astype(jnp.bfloat16)
    resid = (tokens.astype(jnp.float32) + mix_out.astype(jnp.float32)).astype(jnp.bfloat16)
    top = route_ids.shape[1]
    local = expert_gate.shape[0]
    experts = lax.axis_size("ep") * local
    capacity = max(2, 2 * seqs * top // experts)
    flat = route_ids.reshape(-1)
    onehot = (flat[:, None] == jnp.arange(experts, dtype=jnp.int32)[None, :]).astype(jnp.int32)
    before = jnp.cumsum(onehot, axis=0) - onehot
    slot = jnp.sum(before * onehot, axis=1)
    slot_id = slot * experts + flat
    places = jnp.arange(capacity * experts, dtype=jnp.int32)
    hits = slot_id[None, :] == places[:, None]
    dispatch = jnp.sum(
        hits.reshape(capacity * experts, seqs, top).astype(jnp.float32), axis=2
    ).astype(jnp.bfloat16)
    spread = jnp.transpose(hits).reshape(seqs, top, capacity * experts)
    combine = jnp.sum(jnp.where(spread, route_weight[:, :, None], 0.0), axis=1)
    full = gathered_copies(resid, "tp", 1)
    normed2 = rms_rows(full, ffn_gain)
    buffer = jnp.dot(dispatch, normed2, preferred_element_type=jnp.float32).astype(jnp.bfloat16)
    buffer = buffer.reshape(capacity, experts, -1)
    block = lax.all_to_all(buffer, "ep", split_axis=1, concat_axis=1, tiled=True)
    count = block.shape[0]
    width = block.shape[2]
    grid = block.reshape(count, -1, local, width)
    rows = grid[:, :, 0].reshape(-1, width)
    first = jnp.dot(rows, expert_gate[0], preferred_element_type=jnp.float32)
    second = jnp.dot(rows, expert_up[0], preferred_element_type=jnp.float32)
    hidden = (jax.nn.silu(first) * second).astype(jnp.bfloat16)
    term = jnp.dot(hidden, expert_down[0], preferred_element_type=jnp.float32)
    term = lax.optimization_barrier(term.astype(jnp.bfloat16)).astype(jnp.float32)
    summed = sent_and_summed(term.astype(jnp.bfloat16), "tp", 1).astype(jnp.bfloat16)
    results = summed.reshape(count, -1, 1, summed.shape[1])
    answered = results.reshape(count, -1, results.shape[3])
    returned = lax.all_to_all(answered, "ep", split_axis=1, concat_axis=1, tiled=True)
    back = returned.reshape(capacity * experts, -1).astype(jnp.float32)
    moe = jnp.dot(combine, back)
    mixed = (resid.astype(jnp.float32) + moe).astype(jnp.bfloat16)
    return (mixed, state_out)


def solution(mesh):
    placed = (
        P("ep", "tp"),
        P("ep", None, "tp"),
        P("ep", "tp"),
        P(),
        P(),
        P(None, "tp"),
        P(None, "tp"),
        P(None, "tp"),
        P("tp", None, None),
        P("tp", None, None),
        P("tp"),
        P("tp", None),
        P("ep", None, "tp"),
        P("ep", None, "tp"),
        P("ep", "tp", None),
        P("ep", None),
        P("ep", None),
    )
    return jax.shard_map(
        body, mesh=mesh, in_specs=placed, out_specs=(P("ep", "tp"), P("ep", "tp")), check_vma=False
    )
```

profile of v0, /device:TPU:1, one launch (start us, length us, event | category | flops | bytes accessed | tf_op | source)
XLA Modules:
  0.0 109.8 jit_solution(5886516992850330418)
XLA Ops:
  0.6 0.0 copy-start
  0.7 1.5 %broadcast_in_dim.14 = bf16[4,64,256]{2,1,0:T(8,128)(2,1)} broadcast(bf16[64,256]{1,0:T(8,128)(2,1)} %param.17), dimensions={1,2} | broadcast | bytes 163840 | tf_op jit(solution)/shard_map/broadcast_in_dim | solution.py:18
  2.2 4.8 %all-to-all-start = ((bf16[4,64,256]{2,1,0:T(8,128)(2,1)}), bf16[4,64,256]{2,1,0:T(8,128)(2,1)S(1)}, u32[]{:S(2)}, u32[]{:S(2)}) async-start(bf16[4,64,256]{2,1,0:T(8,128)(2,1)} %broadcast_in_dim.14), calls=%async_computation | async-start | bytes 262144 | tf_op jit(solution)/shard_map/all_to_all | solution.py:18
  7.0 0.7 convert_element_type.113
  7.7 0.7 convert_element_type.117
  8.4 0.7 fusion.55
  9.1 0.8 copy.80
  9.8 0.1 eq.37
  10.0 0.0 copy-start.13
  10.0 0.1 fusion.38
  10.1 0.2 reduce_window_sum.11
  10.2 0.2 select_reduce_fusion.1
  10.4 1.4 %all-to-all-done = bf16[4,64,256]{2,1,0:T(8,128)(2,1)S(1)} async-done(((bf16[4,64,256]{2,1,0:T(8,128)(2,1)}), bf16[4,64,256]{2,1,0:T(8,128)(2,1)S(1)}, u32[]{:S(2)}, u32[]{:S(2)}) %all-to-all-start) | async-done | bytes 131104 | tf_op jit(solution)/shard_map/all_to_all | solution.py:18
  11.9 0.1 fusion.34
  12.1 0.2 fusion.27
  12.4 0.1 convert_element_type.119
  12.5 0.1 fusion.24
  12.7 0.1 copy.76
  12.7 0.1 div.24
  12.8 0.1 fusion.20
  13.0 0.1 copy.78
  13.0 0.1 div.26
  13.2 0.0 copy-start.6
  13.2 0.4 convolution_convert_fusion.1
  13.6 0.6 copy.99
  14.3 3.3 %all-to-all-start.1 = ((bf16[4,64,256]{2,1,0:T(8,128)(2,1)}), bf16[4,64,256]{2,1,0:T(8,128)(2,1)S(1)}, u32[]{:S(2)}, u32[]{:S(2)}) async-start(bf16[4,64,256]{2,1,0:T(8,128)(2,1)} %bitcast.58), calls=%async_computation.1 | async-start | bytes 262144 | tf_op jit(solution)/shard_map/all_to_all | solution.py:33
  17.6 0.1 mul.153
  17.7 0.1 copy.81
  17.8 0.0 copy-done.10
  17.8 4.5 %all-to-all-done.1 = bf16[4,64,256]{2,1,0:T(8,128)(2,1)S(1)} async-done(((bf16[4,64,256]{2,1,0:T(8,128)(2,1)}), bf16[4,64,256]{2,1,0:T(8,128)(2,1)S(1)}, u32[]{:S(2)}, u32[]{:S(2)}) %all-to-all-start.1) | async-done | bytes 131104 | tf_op jit(solution)/shard_map/all_to_all | solution.py:33
  22.4 0.6 broadcast_in_dim.22
  23.1 3.3 %all-to-all-start.2 = ((bf16[4,64,256]{2,1,0:T(8,128)(2,1)}), bf16[4,64,256]{2,1,0:T(8,128)(2,1)S(1)}, u32[]{:S(2)}, u32[]{:S(2)}) async-start(bf16[4,64,256]{2,1,0:T(8,128)(2,1)} %broadcast_in_dim.22), calls=%async_computation.2 | async-start | bytes 262144 | tf_op jit(solution)/shard_map/all_to_all | solution.py:18
  26.4 0.1 convert_reduce_fusion
  26.5 4.7 %all-to-all-done.2 = bf16[4,64,256]{2,1,0:T(8,128)(2,1)S(1)} async-done(((bf16[4,64,256]{2,1,0:T(8,128)(2,1)}), bf16[4,64,256]{2,1,0:T(8,128)(2,1)S(1)}, u32[]{:S(2)}, u32[]{:S(2)}) %all-to-all-start.2) | async-done | bytes 131104 | tf_op jit(solution)/shard_map/all_to_all | solution.py:18
  31.3 0.1 fusion.35
  31.4 0.4 convolution_convert_fusion
  31.8 0.5 copy.83
  32.3 41.8 %all_to_all.30 = bf16[2,128,1024]{2,0,1:T(2,128)(2,1)S(1)} all-to-all(bf16[2,128,1024]{2,0,1:T(2,128)(2,1)S(1)} %copy.83), channel_id=1, replica_groups=mesh['ep'=128,'tp'=4] {'ep'}, dimensions={1} | all-to-all | bytes 1048576 | tf_op jit(solution)/shard_map/all_to_all | solution.py:111
  74.1 0.1 copy.84
  74.3 0.6 fusion.4
  74.9 2.4 %fusion.6 = bf16[256,1024]{1,0:T(8,128)(2,1)S(1)} fusion(bf16[1,640,1024]{2,1,0:T(8,128)(2,1)S(1)} %copy-done, bf16[256,1024]{1,0:T(8,128)(2,1)S(1)} %bitcast.62, bf16[1,1024,640]{2,1,0:T(8,128)(2,1)} %param.30, f32[256,640]{1,0:T(8,128)S(1)} %fusion.4), kind=kOutput, calls=%fused_computation.6 | convolution fusion | flops 672333824 | bytes 4325376 | tf_op jit(solution)/shard_map/dot_general | solution.py:119
  77.3 12.2 %all_to_all.31 = bf16[4,256,256]{2,1,0:T(8,128)(2,1)S(1)} all-to-all(bf16[4,256,256]{2,1,0:T(8,128)(2,1)S(1)} %bitcast.64), channel_id=1, replica_groups=mesh['ep'=128,'tp'=4] {'tp'}, dimensions={0} | all-to-all | bytes 1048576 | tf_op jit(solution)/shard_map/all_to_all | solution.py:33
  89.5 0.1 reduce_sum.85
  89.6 0.8 copy.86
  90.4 5.8 %all-to-all-start.5 = ((bf16[2,128,256]{2,0,1:T(2,128)(2,1)}), bf16[2,128,256]{2,0,1:T(2,128)(2,1)S(1)}, u32[]{:S(2)}, u32[]{:S(2)}) async-start(bf16[2,128,256]{2,0,1:T(2,128)(2,1)} %copy.86), calls=%async_computation.5 | async-start | bytes 262144 | tf_op jit(solution)/shard_map/all_to_all | solution.py:124
  96.2 0.1 select_reduce_fusion
  96.3 12.7 %all-to-all-done.5 = bf16[2,128,256]{2,0,1:T(2,128)(2,1)S(1)} async-done(((bf16[2,128,256]{2,0,1:T(2,128)(2,1)}), bf16[2,128,256]{2,0,1:T(2,128)(2,1)S(1)}, u32[]{:S(2)}, u32[]{:S(2)}) %all-to-all-start.5) | async-done | bytes 131104 | tf_op jit(solution)/shard_map/all_to_all | solution.py:124
  109.0 0.8 fusion.25
  (40 shorter events, 0.3 us)
Async XLA Ops:
  0.6 74.2 %copy-start = (bf16[1,640,1024]{2,1,0:T(8,128)(2,1)S(1)}, bf16[1,640,1024]{2,1,0:T(8,128)(2,1)}, u32[]{:S(2)}) copy-start(bf16[1,640,1024]{2,1,0:T(8,128)(2,1)} %param.31) | copy-start | bytes 3932164
  0.6 11.4 %copy-start.4 = (bf16[1024,128]{1,0:T(8,128)(2,1)S(1)}, bf16[1024,128]{1,0:T(8,128)(2,1)}, u32[]{:S(2)}) copy-start(bf16[1024,128]{1,0:T(8,128)(2,1)} %param.22) | copy-start | bytes 786436
  0.7 11.7 %copy-start.7 = (bf16[64,3,128]{2,0,1:T(8,128)(2,1)S(1)}, bf16[64,3,128]{2,0,1:T(8,128)(2,1)}, u32[]{:S(2)}) copy-start(bf16[64,3,128]{2,0,1:T(8,128)(2,1)} %param.18) | copy-start | bytes 147460
  0.7 11.8 %copy-start.12 = (bf16[2,64,64]{2,1,0:T(8,128)(2,1)S(1)}, bf16[2,64,64]{2,1,0:T(8,128)(2,1)}, u32[]{:S(2)}) copy-start(bf16[2,64,64]{2,1,0:T(8,128)(2,1)} %param.25) | copy-start | bytes 49156
  2.2 9.7 %all-to-all-start = ((bf16[4,64,256]{2,1,0:T(8,128)(2,1)}), bf16[4,64,256]{2,1,0:T(8,128)(2,1)S(1)}, u32[]{:S(2)}, u32[]{:S(2)}) async-start(bf16[4,64,256]{2,1,0:T(8,128)(2,1)} %broadcast_in_dim.14), calls=%async_computation | async-start | bytes 262144 | tf_op jit(solution)/shard_map/all_to_all | solution.py:18
  10.0 2.8 %copy-start.13 = (bf16[2,64,64]{2,1,0:T(8,128)(2,1)S(1)}, bf16[2,64,64]{2,1,0:T(8,128)(2,1)}, u32[]{:S(2)}) copy-start(bf16[2,64,64]{2,1,0:T(8,128)(2,1)} %param.26) | copy-start | bytes 49156
  11.9 1.3 %copy-start.8 = (f32[64,128]{1,0:T(8,128)S(1)}, f32[64,128]{1,0:T(8,128)}, u32[]{:S(2)}) copy-start(f32[64,128]{1,0:T(8,128)} %param.19) | copy-start | bytes 98308
  11.9 1.3 %copy-start.2 = (bf16[128,1024]{1,0:T(8,128)(2,1)S(1)}, bf16[128,1024]{1,0:T(8,128)(2,1)}, u32[]{:S(2)}) copy-start(bf16[128,1024]{1,0:T(8,128)(2,1)} %param.28) | copy-start | bytes 786436
  11.9 1.3 %copy-start.3 = (bf16[1024,128]{1,0:T(8,128)(2,1)S(1)}, bf16[1024,128]{1,0:T(8,128)(2,1)}, u32[]{:S(2)}) copy-start(bf16[1024,128]{1,0:T(8,128)(2,1)} %param.23) | copy-start | bytes 786436
  12.6 5.2 %copy-start.9 = (s32[64,2]{0,1:T(2,128)S(1)}, s32[64,2]{0,1:T(2,128)}, u32[]{:S(2)}) copy-start(s32[64,2]{0,1:T(2,128)} %param.32) | copy-start | bytes 1540
  12.6 5.2 %copy-start.10 = (bf16[1024]{0:T(1024)(128)(2,1)S(1)}, bf16[1024]{0:T(1024)(128)(2,1)}, u32[]{:S(2)}) copy-start(bf16[1024]{0:T(1024)(128)(2,1)} %param.21) | copy-start | bytes 6148
  12.6 9.8 %copy-start.5 = (bf16[64,256]{1,0:T(8,128)(2,1)S(1)}, bf16[64,256]{1,0:T(8,128)(2,1)}, u32[]{:S(2)}) copy-start(bf16[64,256]{1,0:T(8,128)(2,1)} %param.17) | copy-start | bytes 98308
  13.2 18.0 %copy-start.6 = (f32[64,128]{1,0:T(8,128)}, f32[64,128]{1,0:T(8,128)S(1)}, u32[]{:S(2)}) copy-start(f32[64,128]{1,0:T(8,128)S(1)} %multiply_add_fusion) | copy-start | bytes 98308
  14.3 8.1 %all-to-all-start.1 = ((bf16[4,64,256]{2,1,0:T(8,128)(2,1)}), bf16[4,64,256]{2,1,0:T(8,128)(2,1)S(1)}, u32[]{:S(2)}, u32[]{:S(2)}) async-start(bf16[4,64,256]{2,1,0:T(8,128)(2,1)} %bitcast.58), calls=%async_computation.1 | async-start | bytes 262144 | tf_op jit(solution)/shard_map/all_to_all | solution.py:33
  23.1 8.1 %all-to-all-start.2 = ((bf16[4,64,256]{2,1,0:T(8,128)(2,1)}), bf16[4,64,256]{2,1,0:T(8,128)(2,1)S(1)}, u32[]{:S(2)}, u32[]{:S(2)}) async-start(bf16[4,64,256]{2,1,0:T(8,128)(2,1)} %broadcast_in_dim.22), calls=%async_computation.2 | async-start | bytes 262144 | tf_op jit(solution)/shard_map/all_to_all | solution.py:18
  32.3 41.9 %copy-start.1 = (bf16[1,1024,640]{2,1,0:T(8,128)(2,1)S(1)}, bf16[1,1024,640]{2,1,0:T(8,128)(2,1)}, u32[]{:S(2)}) copy-start(bf16[1,1024,640]{2,1,0:T(8,128)(2,1)} %param.29) | copy-start | bytes 3932164
  77.3 18.9 %copy-start.11 = (f32[64,2]{0,1:T(2,128)S(1)}, f32[64,2]{0,1:T(2,128)}, u32[]{:S(2)}) copy-start(f32[64,2]{0,1:T(2,128)} %param.33) | copy-start | bytes 1540
  90.4 18.6 %all-to-all-start.5 = ((bf16[2,128,256]{2,0,1:T(2,128)(2,1)}), bf16[2,128,256]{2,0,1:T(2,128)(2,1)S(1)}, u32[]{:S(2)}, u32[]{:S(2)}) async-start(bf16[2,128,256]{2,0,1:T(2,128)(2,1)} %copy.86), calls=%async_computation.5 | async-start | bytes 262144 | tf_op jit(solution)/shard_map/all_to_all | solution.py:124
where the time goes:
time: 110 us
  blocking collectives  54 us (49%)
  waiting for transfers between devices  23.4 us (21%)
  starting transfers between devices  17.3 us (16%)
  local copies, waits for them, and re-layouts  5.92 us (5%)
  matrix products  5.02 us (5%)
  other arithmetic  3.14 us (3%)
    all_to_all x1, blocking collectives, body(): lax.all_to_all(buffer, 'ep', split_axis=1, concat_axis=1, tiled=True)  41.8 us
    all_to_all x1, waiting for transfers between devices, body(): lax.all_to_all(answered, 'ep', split_axis=1, concat_axis=1, tiled=True)  12.7 us
    all_to_all x1, blocking collectives, sent_and_summed(): lax.all_to_all(pieces, axis, split_axis=0, concat_axis=0, tiled=True)  12.2 us
    all_to_all x2, starting transfers between devices, sent_to_all(): lax.all_to_all(jnp.broadcast_to(x[None], (count, *x.shape)), axis, 0, 0,...  8.15 us
    all_to_all x2, waiting for transfers between devices, sent_to_all(): lax.all_to_all(jnp.broadcast_to(x[None], (count, *x.shape)), axis, 0, 0,...  6.13 us
    all_to_all x1, starting transfers between devices, body(): lax.all_to_all(answered, 'ep', split_axis=1, concat_axis=1, tiled=True)  5.77 us
    all_to_all x1, waiting for transfers between devices, sent_and_summed(): lax.all_to_all(pieces, axis, split_axis=0, concat_axis=0, tiled=True)  4.54 us
    all_to_all x1, starting transfers between devices, sent_and_summed(): lax.all_to_all(pieces, axis, split_axis=0, concat_axis=0, tiled=True)  3.32 us
  transfers between devices with their start and end apart: 4, of which 4 were waited for; matrix products, arithmetic and copies ran while one was open for 3% of the time, Pallas kernels for 0%

commit v1 on v0

--- a/solution.py
+++ b/solution.py
@@ -121,7 +121,16 @@
     summed = sent_and_summed(term.astype(jnp.bfloat16), "tp", 1).astype(jnp.bfloat16)
     results = summed.reshape(count, -1, 1, summed.shape[1])
     answered = results.reshape(count, -1, results.shape[3])
-    returned = lax.all_to_all(answered, "ep", split_axis=1, concat_axis=1, tiled=True)
+    track_ports = lambda local_x: jnp.concatenate(
+        jax.lax.all_to_all(
+            jnp.stack(jnp.split(local_x, jax.lax.axis_size("ep"), axis=1)),
+            "ep",
+            split_axis=0,
+            concat_axis=0,
+        ),
+        axis=1,
+    )
+    returned = track_ports(answered)
     back = returned.reshape(capacity * experts, -1).astype(jnp.float32)
     moe = jnp.dot(combine, back)
     mixed = (resid.astype(jnp.float32) + moe).astype(jnp.bfloat16)

time: 110 us -> 184 us (1.67)
  local copies, waits for them, and re-layouts: 5.92 us -> 79.4 us
    unnamed x29 -> x156, local copies, waits for them, and re-layouts: 0.87 us -> 73.8 us
  transfers between devices with their start and end apart: 4 -> 4, of which waited for: 4 -> 4; matrix products, arithmetic and copies ran while one was open for 3% -> 2% of each run, Pallas kernels for 0% -> 0%
where the time goes in v1:
time: 184 us; the launch traced here: 183 us
  local copies, waits for them, and re-layouts  79.4 us (43%)
  blocking collectives  54 us (29%)
  waiting for transfers between devices  23.4 us (13%)
  starting transfers between devices  17.2 us (9%)
  matrix products  5.03 us (3%)
  other arithmetic  3.14 us (2%)
    unnamed x156, local copies, waits for them, and re-layouts  73.8 us
    all_to_all x1, blocking collectives, body(): lax.all_to_all(buffer, 'ep', split_axis=1, concat_axis=1, tiled=True)  41.8 us
    all_to_all x1, waiting for transfers between devices, body(): jax.lax.all_to_all(jnp.stack(jnp.split(local_x, jax.lax.axis_size('ep'),...  12.7 us
    all_to_all x1, blocking collectives, sent_and_summed(): lax.all_to_all(pieces, axis, split_axis=0, concat_axis=0, tiled=True)  12.2 us
    all_to_all x2, starting transfers between devices, sent_to_all(): lax.all_to_all(jnp.broadcast_to(x[None], (count, *x.shape)), axis, 0, 0,...  8.15 us
    all_to_all x2, waiting for transfers between devices, sent_to_all(): lax.all_to_all(jnp.broadcast_to(x[None], (count, *x.shape)), axis, 0, 0,...  6.13 us
    all_to_all x1, starting transfers between devices, body(): jax.lax.all_to_all(jnp.stack(jnp.split(local_x, jax.lax.axis_size('ep'),...  5.75 us
    all_to_all x1, waiting for transfers between devices, sent_and_summed(): lax.all_to_all(pieces, axis, split_axis=0, concat_axis=0, tiled=True)  4.54 us
  transfers between devices with their start and end apart: 4, of which 4 were waited for; matrix products, arithmetic and copies ran while one was open for 2% of the time, Pallas kernels for 0%

profile of v1, /device:TPU:1, one launch (start us, length us, event | category | flops | bytes accessed | tf_op | source)
XLA Modules:
  0.0 183.4 jit_solution(1384869663402579028)
XLA Ops:
  0.7 1.5 broadcast_in_dim.14
  2.2 4.8 %all-to-all-start = ((bf16[4,64,256]{2,1,0:T(8,128)(2,1)}), bf16[4,64,256]{2,1,0:T(8,128)(2,1)S(1)}, u32[]{:S(2)}, u32[]{:S(2)}) async-start(bf16[4,64,256]{2,1,0:T(8,128)(2,1)} %broadcast_in_dim.14), calls=%async_computation | async-start | bytes 262144 | tf_op jit(solution)/shard_map/all_to_all | solution.py:18
  7.0 0.7 convert_element_type.113
  7.7 0.7 convert_element_type.117
  8.4 0.7 fusion.55
  9.1 0.8 copy.3682
  10.4 1.4 all-to-all-done
  13.7 0.7 copy.3681
  14.4 3.3 %all-to-all-start.1 = ((bf16[4,64,256]{2,1,0:T(8,128)(2,1)}), bf16[4,64,256]{2,1,0:T(8,128)(2,1)S(1)}, u32[]{:S(2)}, u32[]{:S(2)}) async-start(bf16[4,64,256]{2,1,0:T(8,128)(2,1)} %copy.3681), calls=%async_computation.1 | async-start | bytes 262144 | tf_op jit(solution)/shard_map/all_to_all | solution.py:33
  17.9 4.5 %all-to-all-done.1 = bf16[4,64,256]{2,1,0:T(8,128)(2,1)S(1)} async-done(((bf16[4,64,256]{2,1,0:T(8,128)(2,1)}), bf16[4,64,256]{2,1,0:T(8,128)(2,1)S(1)}, u32[]{:S(2)}, u32[]{:S(2)}) %all-to-all-start.1) | async-done | bytes 131104 | tf_op jit(solution)/shard_map/all_to_all | solution.py:33
  22.5 0.7 broadcast_in_dim.22
  23.2 3.3 %all-to-all-start.2 = ((bf16[4,64,256]{2,1,0:T(8,128)(2,1)}), bf16[4,64,256]{2,1,0:T(8,128)(2,1)S(1)}, u32[]{:S(2)}, u32[]{:S(2)}) async-start(bf16[4,64,256]{2,1,0:T(8,128)(2,1)} %broadcast_in_dim.22), calls=%async_computation.2 | async-start | bytes 262144 | tf_op jit(solution)/shard_map/all_to_all | solution.py:18
  26.6 4.7 %all-to-all-done.2 = bf16[4,64,256]{2,1,0:T(8,128)(2,1)S(1)} async-done(((bf16[4,64,256]{2,1,0:T(8,128)(2,1)}), bf16[4,64,256]{2,1,0:T(8,128)(2,1)S(1)}, u32[]{:S(2)}, u32[]{:S(2)}) %all-to-all-start.2) | async-done | bytes 131104 | tf_op jit(solution)/shard_map/all_to_all | solution.py:18
  32.4 41.8 %all_to_all.30 = bf16[2,128,1024]{2,0,1:T(2,128)(2,1)S(1)} all-to-all(bf16[2,128,1024]{2,0,1:T(2,128)(2,1)S(1)} %copy.3685), channel_id=1, replica_groups=mesh['ep'=128,'tp'=4] {'ep'}, dimensions={1} | all-to-all | bytes 1048576 | tf_op jit(solution)/shard_map/all_to_all | solution.py:111
  75.0 2.4 %fusion.6 = bf16[256,1024]{1,0:T(8,128)(2,1)S(1)} fusion(bf16[1,640,1024]{2,1,0:T(8,128)(2,1)S(1)} %copy-done, bf16[256,1024]{1,0:T(8,128)(2,1)S(1)} %bitcast.307, bf16[1,1024,640]{2,1,0:T(8,128)(2,1)} %param.30, f32[256,640]{1,0:T(8,128)S(1)} %fusion.4), kind=kOutput, calls=%fused_computation.6 | convolution fusion | flops 672333824 | bytes 4325376 | tf_op jit(solution)/shard_map/dot_general | solution.py:119
  77.8 12.2 %all_to_all.31 = bf16[4,256,256]{2,1,0:T(8,128)(2,1)S(1)} all-to-all(bf16[4,256,256]{2,1,0:T(8,128)(2,1)S(1)} %copy.3687), channel_id=1, replica_groups=mesh['ep'=128,'tp'=4] {'tp'}, dimensions={0} | all-to-all | bytes 1048576 | tf_op jit(solution)/shard_map/all_to_all | solution.py:33
  91.6 0.6 constant_dynamic-update-slice_fusion.125
  92.2 0.6 constant_dynamic-update-slice_fusion.124
  93.9 0.6 constant_dynamic-update-slice_fusion.121
  100.8 0.6 constant_dynamic-update-slice_fusion.109
  103.6 0.6 constant_dynamic-update-slice_fusion.104
  104.2 0.6 constant_dynamic-update-slice_fusion.103
  106.5 0.6 constant_dynamic-update-slice_fusion.99
  107.1 0.6 constant_dynamic-update-slice_fusion.98
  110.0 0.6 constant_dynamic-update-slice_fusion.93
  110.6 0.6 constant_dynamic-update-slice_fusion.92
  112.9 0.6 constant_dynamic-update-slice_fusion.88
  118.6 0.6 constant_dynamic-update-slice_fusion.78
  124.4 0.6 constant_dynamic-update-slice_fusion.68
  126.1 0.6 constant_dynamic-update-slice_fusion.65
  126.7 0.6 constant_dynamic-update-slice_fusion.64
  127.3 0.6 constant_dynamic-update-slice_fusion.63
  127.9 0.6 constant_dynamic-update-slice_fusion.62
  129.6 0.6 constant_dynamic-update-slice_fusion.59
  130.2 0.6 constant_dynamic-update-slice_fusion.58
  133.7 0.6 constant_dynamic-update-slice_fusion.52
  139.3 0.6 constant_dynamic-update-slice_fusion.42
  140.5 0.6 constant_dynamic-update-slice_fusion.40
  144.5 0.6 constant_dynamic-update-slice_fusion.33
  146.3 0.6 constant_dynamic-update-slice_fusion.30
  148.0 0.6 constant_dynamic-update-slice_fusion.27
  152.0 0.6 constant_dynamic-update-slice_fusion.20
  158.9 0.6 constant_dynamic-update-slice_fusion.8
  161.7 0.6 constant_dynamic-update-slice_fusion.3
  162.3 0.6 constant_dynamic-update-slice_fusion.2
  164.1 5.8 %all-to-all-start.5 = ((bf16[128,2,1,256]{3,1,2,0:T(2,128)(2,1)}), bf16[128,2,1,256]{3,1,2,0:T(2,128)(2,1)S(1)}, u32[]{:S(2)}, u32[]{:S(2)}) async-start(bf16[128,2,1,256]{3,1,2,0:T(2,128)(2,1)} %constant_dynamic-update-slice_fusion), calls=%async_computation.5 | async-start | bytes 262144 | tf_op jit(solution)/shard_map/all_to_all | solution.py:125
  169.9 12.7 %all-to-all-done.5 = bf16[128,2,1,256]{3,1,2,0:T(2,128)(2,1)S(1)} async-done(((bf16[128,2,1,256]{3,1,2,0:T(2,128)(2,1)}), bf16[128,2,1,256]{3,1,2,0:T(2,128)(2,1)S(1)}, u32[]{:S(2)}, u32[]{:S(2)}) %all-to-all-start.5) | async-done | bytes 131104 | tf_op jit(solution)/shard_map/all_to_all | solution.py:125
  182.7 0.8 fusion.25
  (176 shorter events, 61.6 us)
Async XLA Ops:
  0.6 74.3 %copy-start = (bf16[1,640,1024]{2,1,0:T(8,128)(2,1)S(1)}, bf16[1,640,1024]{2,1,0:T(8,128)(2,1)}, u32[]{:S(2)}) copy-start(bf16[1,640,1024]{2,1,0:T(8,128)(2,1)} %param.31) | copy-start | bytes 3932164
  0.6 11.4 %copy-start.4 = (bf16[1024,128]{1,0:T(8,128)(2,1)S(1)}, bf16[1024,128]{1,0:T(8,128)(2,1)}, u32[]{:S(2)}) copy-start(bf16[1024,128]{1,0:T(8,128)(2,1)} %param.22) | copy-start | bytes 786436
  0.7 11.7 %copy-start.7 = (bf16[64,3,128]{2,0,1:T(8,128)(2,1)S(1)}, bf16[64,3,128]{2,0,1:T(8,128)(2,1)}, u32[]{:S(2)}) copy-start(bf16[64,3,128]{2,0,1:T(8,128)(2,1)} %param.18) | copy-start | bytes 147460
  0.7 11.8 %copy-start.12 = (bf16[2,64,64]{2,1,0:T(8,128)(2,1)S(1)}, bf16[2,64,64]{2,1,0:T(8,128)(2,1)}, u32[]{:S(2)}) copy-start(bf16[2,64,64]{2,1,0:T(8,128)(2,1)} %param.25) | copy-start | bytes 49156
  2.2 9.7 %all-to-all-start = ((bf16[4,64,256]{2,1,0:T(8,128)(2,1)}), bf16[4,64,256]{2,1,0:T(8,128)(2,1)S(1)}, u32[]{:S(2)}, u32[]{:S(2)}) async-start(bf16[4,64,256]{2,1,0:T(8,128)(2,1)} %broadcast_in_dim.14), calls=%async_computation | async-start | bytes 262144 | tf_op jit(solution)/shard_map/all_to_all | solution.py:18
  10.0 2.8 %copy-start.13 = (bf16[2,64,64]{2,1,0:T(8,128)(2,1)S(1)}, bf16[2,64,64]{2,1,0:T(8,128)(2,1)}, u32[]{:S(2)}) copy-start(bf16[2,64,64]{2,1,0:T(8,128)(2,1)} %param.26) | copy-start | bytes 49156
  11.9 1.2 copy-start.8
  11.9 1.3 copy-start.2
  11.9 1.3 copy-start.3
  12.7 5.2 %copy-start.9 = (s32[64,2]{0,1:T(2,128)S(1)}, s32[64,2]{0,1:T(2,128)}, u32[]{:S(2)}) copy-start(s32[64,2]{0,1:T(2,128)} %param.32) | copy-start | bytes 1540
  12.7 5.2 %copy-start.10 = (bf16[1024]{0:T(1024)(128)(2,1)S(1)}, bf16[1024]{0:T(1024)(128)(2,1)}, u32[]{:S(2)}) copy-start(bf16[1024]{0:T(1024)(128)(2,1)} %param.21) | copy-start | bytes 6148
  12.8 9.7 %copy-start.5 = (bf16[64,256]{1,0:T(8,128)(2,1)S(1)}, bf16[64,256]{1,0:T(8,128)(2,1)}, u32[]{:S(2)}) copy-start(bf16[64,256]{1,0:T(8,128)(2,1)} %param.17) | copy-start | bytes 98308
  13.2 18.1 %copy-start.6 = (f32[64,128]{1,0:T(8,128)}, f32[64,128]{1,0:T(8,128)S(1)}, u32[]{:S(2)}) copy-start(f32[64,128]{1,0:T(8,128)S(1)} %multiply_add_fusion) | copy-start | bytes 98308
  14.4 8.1 %all-to-all-start.1 = ((bf16[4,64,256]{2,1,0:T(8,128)(2,1)}), bf16[4,64,256]{2,1,0:T(8,128)(2,1)S(1)}, u32[]{:S(2)}, u32[]{:S(2)}) async-start(bf16[4,64,256]{2,1,0:T(8,128)(2,1)} %copy.3681), calls=%async_computation.1 | async-start | bytes 262144 | tf_op jit(solution)/shard_map/all_to_all | solution.py:33
  23.2 8.1 %all-to-all-start.2 = ((bf16[4,64,256]{2,1,0:T(8,128)(2,1)}), bf16[4,64,256]{2,1,0:T(8,128)(2,1)S(1)}, u32[]{:S(2)}, u32[]{:S(2)}) async-start(bf16[4,64,256]{2,1,0:T(8,128)(2,1)} %broadcast_in_dim.22), calls=%async_computation.2 | async-start | bytes 262144 | tf_op jit(solution)/shard_map/all_to_all | solution.py:18
  32.4 41.9 %copy-start.1 = (bf16[1,1024,640]{2,1,0:T(8,128)(2,1)S(1)}, bf16[1,1024,640]{2,1,0:T(8,128)(2,1)}, u32[]{:S(2)}) copy-start(bf16[1,1024,640]{2,1,0:T(8,128)(2,1)} %param.29) | copy-start | bytes 3932164
  77.8 92.0 %copy-start.11 = (f32[64,2]{0,1:T(2,128)S(1)}, f32[64,2]{0,1:T(2,128)}, u32[]{:S(2)}) copy-start(f32[64,2]{0,1:T(2,128)} %param.33) | copy-start | bytes 1540
  164.1 18.6 %all-to-all-start.5 = ((bf16[128,2,1,256]{3,1,2,0:T(2,128)(2,1)}), bf16[128,2,1,256]{3,1,2,0:T(2,128)(2,1)S(1)}, u32[]{:S(2)}, u32[]{:S(2)}) async-start(bf16[128,2,1,256]{3,1,2,0:T(2,128)(2,1)} %constant_dynamic-update-slice_fusion), calls=%async_computation.5 | async-start | bytes 262144 | tf_op jit(solution)/shard_map/all_to_all | solution.py:125
